TPU v7x, 32 devices: a whole 2x2x4 slice. The times are simulated.
32 devices in a mesh: row: 8 (over z, x), col: 4 (over y, core).
Axes of the slice: x: 2, y: 2, z: 4, core: 2. Of those that a mesh axis runs over, the one named last changes fastest.
Arguments:
- tokens: bfloat16 [16384, 4096], P(('row', 'col')), may hold values from -36 to 36
- norm_gain: bfloat16 [4096], replicated, may hold values from 0.099609375 to 1.8984375
- in_weight: bfloat16 [4096, 1024], replicated, may hold values from -0.09375 to 0.09375
- out_weight: bfloat16 [1024, 4096], replicated, may hold values from -0.1875 to 0.1875
Outputs:
- mixed: bfloat16 [16384, 4096], P(('row', 'col'))
All inputs are finite; a program needn't handle non-finite values.
Results may differ from a plain program's by a relative error of at most 0.0071.
Values may be sent and summed in bfloat16 or wider, within the bound.
A program may use at most 128 MiB of HBM per device.

v0:
```python
import math

import jax
import jax.numpy as jnp
from jax import lax
from jax.sharding import PartitionSpec as P

GROUP_WIDTH = 64
FACTOR = 256


highest = lax.Precision.HIGHEST


def dft_tables(count, scaling):
    first_index = lax.broadcasted_iota(jnp.int32, (count, count), 0)
    second_index = lax.broadcasted_iota(jnp.int32, (count, count), 1)
    angles = 2.0 * math.pi / count * (first_index * second_index % count).astype(jnp.float32)
    return (jnp.cos(angles) * scaling, jnp.sin(angles) * scaling)


def position_transform(real_part, imag_part, length, factor):
    columns = real_part.shape[0]
    remain = length // factor
    real_grid = real_part.reshape(columns, factor, remain)
    imag_grid = imag_part.reshape(columns, factor, remain)
    outer_cos, outer_sin = dft_tables(factor, 1.0)
    real_one = jnp.einsum("kn,cnm->ckm", outer_cos, real_grid, precision=highest) + jnp.einsum(
        "kn,cnm->ckm", outer_sin, imag_grid, precision=highest
    )
    imag_one = jnp.einsum("kn,cnm->ckm", outer_cos, imag_grid, precision=highest) - jnp.einsum(
        "kn,cnm->ckm", outer_sin, real_grid, precision=highest
    )
    outer_index = lax.broadcasted_iota(jnp.int32, (factor, remain), 0)
    inner_index = lax.broadcasted_iota(jnp.int32, (factor, remain), 1)
    angles = 2.0 * math.pi / length * (outer_index * inner_index).astype(jnp.float32)
    twist_cos = jnp.cos(angles)
    twist_sin = jnp.sin(angles)
    real_two = real_one * twist_cos + imag_one * twist_sin
    imag_two = imag_one * twist_cos - real_one * twist_sin
    inner_cos, inner_sin = dft_tables(remain, 1.0 / math.sqrt(length))
    real_out = jnp.einsum("ckn,nq->cqk", real_two, inner_cos, precision=highest) + jnp.einsum(
        "ckn,nq->cqk", imag_two, inner_sin, precision=highest
    )
    real_out = real_out.reshape(columns, length)
    return (real_out, real_out)


def local(tokens, norm_gain, in_weight, out_weight):
    rows_here = tokens.shape[0]
    channels = in_weight.shape[1]
    groups = channels // GROUP_WIDTH
    devices = lax.axis_size(("row", "col"))
    length = rows_here * devices
    floats = tokens.astype(jnp.float32)
    scaling = lax.rsqrt(jnp.mean(floats * floats, axis=-1, keepdims=True) + 1e-06)
    normed = (floats * scaling * norm_gain.astype(jnp.float32)).astype(jnp.bfloat16)
    hidden = lax.dot_general(
        in_weight, normed, (((0,), (1,)), ((), ())), preferred_element_type=jnp.float32
    ).astype(jnp.bfloat16)
    widened = (
        lax.optimization_barrier(hidden).astype(jnp.float32).reshape(groups, GROUP_WIDTH, rows_here)
    )
    channel_scale = 1.0 / math.sqrt(GROUP_WIDTH)
    chan_cos, chan_sin = dft_tables(GROUP_WIDTH, channel_scale)
    real_chan = jnp.einsum("mc,gct->gmt", chan_cos, widened, precision=highest).reshape(
        channels, rows_here
    )
    imag_chan = -jnp.einsum("mc,gct->gmt", chan_sin, widened, precision=highest).reshape(
        channels, rows_here
    )
    real_cols, imag_cols = (
        lax.all_to_all(
            real_chan.astype(jnp.bfloat16), ("row", "col"), split_axis=0, concat_axis=1, tiled=True
        ),
        lax.all_to_all(
            imag_chan.astype(jnp.bfloat16), ("row", "col"), split_axis=0, concat_axis=1, tiled=True
        ),
    )
    real_out, unused_imag = position_transform(
        real_cols.astype(jnp.float32), imag_cols.astype(jnp.float32), length, FACTOR
    )
    outgoing = real_out.astype(jnp.bfloat16)
    returned = lax.all_to_all(outgoing, ("row", "col"), split_axis=1, concat_axis=0, tiled=True)
    mixed = lax.dot_general(
        returned, out_weight, (((0,), (0,)), ((), ())), preferred_element_type=jnp.float32
    )
    return mixed.astype(jnp.bfloat16)


def solution(mesh):
    placed = (P(("row", "col"), None), P(), P(), P())
    return jax.shard_map(
        local, mesh=mesh, in_specs=placed, out_specs=P(("row", "col"), None), check_vma=False
    )
```

profile of v0, /device:TPU:0, one launch (start us, length us, event | category | flops | bytes accessed | tf_op | source)
XLA Modules:
  0.0 136.7 jit_solution(4453239645320215439)
XLA Ops:
  0.0 0.7 convert_element_type.88
  0.7 0.0 copy-start.2
  0.7 3.2 %fusion = f32[512]{0:T(512)S(1)} fusion(bf16[512,4096]{1,0:T(8,128)(2,1)} %param.4), kind=kLoop, calls=%fused_computation.2 | loop fusion | flops 6290944 | bytes 4196352 | tf_op jit(solution)/shard_map/reduce_sum | solution.py:56
  3.9 0.2 copy-done.2
  4.1 7.2 %fusion.18 = bf16[1024,512]{0,1:T(8,128)(2,1)S(1)} fusion(bf16[4096,1024]{1,0:T(8,128)(2,1)} %param.6, bf16[512,4096]{1,0:T(8,128)(2,1)S(1)} %copy-done.2, f32[4096]{0:T(1024)S(1)} %convert_element_type.88, f32[512]{0:T(512)S(1)} %add_rsqrt_fusion), kind=kOutput, calls=%fused_computation.23 | convolution fusion | flops 4303880192 | bytes 13649920 | tf_op jit(solution)/shard_map/dot_general | solution.py:58
  11.3 0.5 copy.19
  11.9 2.1 %convolution_convert_fusion.1 = bf16[16,512,64]{1,2,0:T(8,128)(2,1)} fusion(bf16[16,64,512]{2,1,0:T(8,128)(2,1)S(1)} %bitcast.73), kind=kOutput, calls=%fused_computation.22 | convolution fusion | flops 403238912 | bytes 2097152 | tf_op jit(solution)/shard_map/mc,gct->gmt/dot_general | solution.py:66
  14.0 7.3 %all-to-all-start = ((bf16[32,32,512]{2,1,0:T(8,128)(2,1)}), bf16[32,32,512]{2,1,0:T(8,128)(2,1)S(1)}, u32[]{:S(2)}, u32[]{:S(2)}) async-start(bf16[32,32,512]{2,1,0:T(8,128)(2,1)} %bitcast.5), calls=%async_computation | async-start | bytes 2097152 | tf_op jit(solution)/shard_map/all_to_all | solution.py:73
  21.4 2.2 %negate_convert_fusion = bf16[16,512,64]{1,2,0:T(8,128)(2,1)} fusion(bf16[16,64,512]{2,1,0:T(8,128)(2,1)S(1)} %bitcast.74), kind=kOutput, calls=%fused_computation.18 | convolution fusion | flops 403763200 | bytes 2097152 | tf_op jit(solution)/shard_map/mc,gct->gmt/dot_general | solution.py:69
  23.6 24.0 %all-to-all-done = bf16[32,32,512]{2,1,0:T(8,128)(2,1)S(1)} async-done(((bf16[32,32,512]{2,1,0:T(8,128)(2,1)}), bf16[32,32,512]{2,1,0:T(8,128)(2,1)S(1)}, u32[]{:S(2)}, u32[]{:S(2)}) %all-to-all-start) | async-done | bytes 1048608 | tf_op jit(solution)/shard_map/all_to_all | solution.py:73
  47.6 3.7 %all-to-all-start.1 = ((bf16[32,32,512]{2,1,0:T(8,128)(2,1)}), bf16[32,32,512]{2,1,0:T(8,128)(2,1)}, u32[]{:S(2)}, u32[]{:S(2)}) async-start(bf16[32,32,512]{2,1,0:T(8,128)(2,1)} %bitcast.10), calls=%async_computation.1 | async-start | bytes 2097152 | tf_op jit(solution)/shard_map/all_to_all | solution.py:76
  51.3 0.2 fusion.46
  51.6 0.6 copy.21
  52.2 1.1 reshape.55
  53.3 4.2 %fusion.35 = f32[32,64,256]{2,1,0:T(8,128)} fusion(bf16[32,256,64]{2,1,0:T(8,128)(2,1)S(1)} %reshape.55), kind=kOutput, calls=%fused_computation.39 | convolution fusion | flops 1611530240 | bytes 3145728 | tf_op jit(solution)/shard_map/kn,cnm->ckm/dot_general | solution.py:28
  57.5 20.0 %all-to-all-done.1 = bf16[32,32,512]{2,1,0:T(8,128)(2,1)} async-done(((bf16[32,32,512]{2,1,0:T(8,128)(2,1)}), bf16[32,32,512]{2,1,0:T(8,128)(2,1)}, u32[]{:S(2)}, u32[]{:S(2)}) %all-to-all-start.1) | async-done | bytes 1048608 | tf_op jit(solution)/shard_map/all_to_all | solution.py:76
  77.5 1.8 %copy.24 = bf16[32,32,512]{2,1,0:T(8,128)(2,1)S(1)} copy(bf16[32,32,512]{2,0,1:T(8,128)(2,1)} %bitcast.11) | data formatting | bytes 2097152 | tf_op jit(solution)/shard_map/all_to_all | solution.py:76
  79.3 2.1 %reshape.56 = bf16[32,256,64]{2,1,0:T(8,128)(2,1)} reshape(bf16[32,32,512]{2,1,0:T(8,128)(2,1)S(1)} %copy.24) | data formatting | bytes 2097152 | tf_op jit(solution)/shard_map/reshape | solution.py:26
  81.4 0.0 copy-start
  81.4 0.0 copy-start.1
  81.4 4.7 %fusion.33 = f32[32,64,256]{2,1,0:T(8,128)S(1)} fusion(bf16[32,256,64]{2,1,0:T(8,128)(2,1)} %reshape.56), kind=kOutput, calls=%fused_computation.37 | convolution fusion | flops 1611530240 | bytes 3145728 | tf_op jit(solution)/shard_map/kn,cnm->ckm/dot_general | solution.py:31
  86.0 0.0 copy-done
  86.1 0.0 copy-done.1
  86.1 2.9 %convolution_add_fusion = f32[32,64,256]{2,1,0:T(8,128)S(1)} fusion(f32[32,64,256]{2,1,0:T(8,128)S(1)} %copy-done.1, bf16[32,256,64]{2,1,0:T(8,128)(2,1)S(1)} %copy-done), kind=kOutput, calls=%fused_computation.20 | convolution fusion | flops 1612054528 | bytes 5242880 | tf_op jit(solution)/shard_map/kn,cnm->ckm/dot_general | solution.py:28
  89.0 2.9 %convolution_subtract_fusion = f32[32,64,256]{2,1,0:T(8,128)S(1)} fusion(f32[32,64,256]{2,1,0:T(8,128)S(1)} %fusion.33, bf16[32,256,64]{2,1,0:T(8,128)(2,1)S(1)} %reshape.55), kind=kOutput, calls=%fused_computation.19 | convolution fusion | flops 1612054528 | bytes 5242880 | tf_op jit(solution)/shard_map/kn,cnm->ckm/dot_general | solution.py:31
  92.0 2.1 %fusion.8 = f32[64,32,256]{2,0,1:T(8,128)S(1)} fusion(f32[32,64,256]{2,1,0:T(8,128)S(1)} %convolution_subtract_fusion, f32[32,64,256]{2,1,0:T(8,128)S(1)} %convolution_add_fusion, f32[256,64]{0,1:T(8,128)S(1)} %get-tuple-element.5, f32[256,64]{0,1:T(8,128)S(1)} %get-tuple-element.6), kind=kOutput, calls=%fused_computation.12 | convolution fusion | flops 404287488 | bytes 6422528 | tf_op jit(solution)/shard_map/ckn,nq->cqk/dot_general | solution.py:42
  94.1 2.5 %fusion.21 = bf16[32,64,256]{2,1,0:T(8,128)(2,1)S(1)} fusion(f32[64,32,256]{2,0,1:T(8,128)S(1)} %fusion.8, f32[32,64,256]{2,1,0:T(8,128)S(1)} %convolution_subtract_fusion, f32[32,64,256]{2,1,0:T(8,128)S(1)} %convolution_add_fusion, f32[256,64]{0,1:T(8,128)S(1)} %get-tuple-element.5, f32[256,64]{0,1:T(8,128)S(1)} %get-tuple-element.6), kind=kOutput, calls=%fused_computation.24 | convolution fusion | flops 405336064 | bytes 7471104 | tf_op jit(solution)/shard_map/ckn,nq->cqk/dot_general | solution.py:42
  96.5 0.4 convert_element_type.102
  96.9 0.6 copy.28
  97.5 29.6 %all_to_all.42 = bf16[32,32,512]{2,0,1:T(8,128)(2,1)S(1)} all-to-all(bf16[32,32,512]{2,0,1:T(8,128)(2,1)S(1)} %copy.28), channel_id=1, replica_groups=mesh['row'=8,'col'=4] {'row','col'}, dimensions={1} | all-to-all | bytes 2097152 | tf_op jit(solution)/shard_map/all_to_all | solution.py:84
  127.2 9.5 %convolution_convert_fusion = bf16[512,4096]{1,0:T(8,128)(2,1)} fusion(bf16[1024,512]{1,0:T(8,128)(2,1)S(1)} %bitcast.76, bf16[1024,4096]{1,0:T(8,128)(2,1)} %param.7), kind=kOutput, calls=%fused_computation.5 | convolution fusion | flops 4297064448 | bytes 13631488 | tf_op jit(solution)/shard_map/dot_general | solution.py:85
  (1 shorter events, 0.0 us)
Async XLA Ops:
  0.7 3.4 %copy-start.2 = (bf16[512,4096]{1,0:T(8,128)(2,1)S(1)}, bf16[512,4096]{1,0:T(8,128)(2,1)}, u32[]{:S(2)}) copy-start(bf16[512,4096]{1,0:T(8,128)(2,1)} %param.4) | copy-start | bytes 12582916
  14.0 33.5 %all-to-all-start = ((bf16[32,32,512]{2,1,0:T(8,128)(2,1)}), bf16[32,32,512]{2,1,0:T(8,128)(2,1)S(1)}, u32[]{:S(2)}, u32[]{:S(2)}) async-start(bf16[32,32,512]{2,1,0:T(8,128)(2,1)} %bitcast.5), calls=%async_computation | async-start | bytes 2097152 | tf_op jit(solution)/shard_map/all_to_all | solution.py:73
  47.6 29.9 %all-to-all-start.1 = ((bf16[32,32,512]{2,1,0:T(8,128)(2,1)}), bf16[32,32,512]{2,1,0:T(8,128)(2,1)}, u32[]{:S(2)}, u32[]{:S(2)}) async-start(bf16[32,32,512]{2,1,0:T(8,128)(2,1)} %bitcast.10), calls=%async_computation.1 | async-start | bytes 2097152 | tf_op jit(solution)/shard_map/all_to_all | solution.py:76
  81.4 4.7 %copy-start = (bf16[32,256,64]{2,1,0:T(8,128)(2,1)S(1)}, bf16[32,256,64]{2,1,0:T(8,128)(2,1)}, u32[]{:S(2)}) copy-start(bf16[32,256,64]{2,1,0:T(8,128)(2,1)} %reshape.56) | copy-start | bytes 3145732
  81.4 4.7 %copy-start.1 = (f32[32,64,256]{2,1,0:T(8,128)S(1)}, f32[32,64,256]{2,1,0:T(8,128)}, u32[]{:S(2)}) copy-start(f32[32,64,256]{2,1,0:T(8,128)} %fusion.35) | copy-start | bytes 6291460
where the time goes:
time: 137 us
  waiting for transfers between devices  44 us (32%)
  matrix products  40.4 us (29%)
  blocking collectives  29.6 us (22%)
  starting transfers between devices  11.1 us (8%)
  local copies, waits for them, and re-layouts  7.3 us (5%)
  other arithmetic  4.19 us (3%)
    all_to_all x1, blocking collectives, local(): lax.all_to_all(outgoing, ('row', 'col'), split_axis=1, concat_axis=0, til...  29.6 us
    all_to_all x1, waiting for transfers between devices, local(): lax.all_to_all(real_chan.astype(jnp.bfloat16), ('row', 'col'), split_axis...  24 us
    all_to_all x1, waiting for transfers between devices, local(): lax.all_to_all(imag_chan.astype(jnp.bfloat16), ('row', 'col'), split_axis...  20 us
    dot_general x1, matrix products, local(): lax.dot_general(returned, out_weight, (((0,), (0,)), ((), ())), preferred...  9.49 us
    all_to_all x1, starting transfers between devices, local(): lax.all_to_all(real_chan.astype(jnp.bfloat16), ('row', 'col'), split_axis...  7.31 us
    dot_general x1, matrix products, local(): lax.dot_general(in_weight, normed, (((0,), (1,)), ((), ())), preferred_el...  7.19 us
    dot_general x1, matrix products, position_transform(): jnp.einsum('kn,cnm->ckm', outer_cos, imag_grid, precision=highest)  4.66 us
    dot_general x1, matrix products, position_transform(): jnp.einsum('kn,cnm->ckm', outer_cos, real_grid, precision=highest)  4.23 us
  transfers between devices with their start and end apart: 2, of which 2 were waited for; matrix products, arithmetic and copies ran while one was open for 6% of the time, Pallas kernels for 0%

commit v1 on v0

v1 whole, which is shorter than its diff:
```python
import functools
import math

import jax
import jax.numpy as jnp
import numpy as np
from jax import lax
from jax.experimental import pallas as pl
from jax.experimental.pallas import tpu as pltpu
from jax.sharding import PartitionSpec as P

GROUP_WIDTH = 64
AXES = ("row", "col")


def channel_tables(slots):
    pairs = slots // 2
    half = GROUP_WIDTH // 2
    index = np.arange(GROUP_WIDTH)
    forward = np.zeros((GROUP_WIDTH, GROUP_WIDTH))
    order = np.zeros((GROUP_WIDTH, GROUP_WIDTH))
    for slot in range(GROUP_WIDTH):
        place, within = divmod(slot, slots)
        pair = place * pairs + within % pairs
        angles = 2.0 * math.pi / GROUP_WIDTH * (pair * index % GROUP_WIDTH)
        if within < pairs:
            forward[slot] = np.cos(angles)
            order[pair, slot] = 1.0
        elif pair == 0:
            forward[slot] = np.cos(math.pi * index)
            order[half, slot] = 1.0
        else:
            forward[slot] = np.sin(angles)
            order[GROUP_WIDTH - pair, slot] = 1.0
    forward /= math.sqrt(GROUP_WIDTH)
    return forward.astype(jnp.bfloat16), order.astype(jnp.bfloat16)


def position_tables(outer, inner):
    length = outer * inner
    k1 = np.arange(outer)
    n2 = np.arange(inner)
    one = 2.0 * math.pi / outer * (np.outer(k1, k1) % outer)
    first = np.concatenate([np.cos(one), -np.sin(one)], axis=1)
    turn = 2.0 * math.pi / length * np.outer(n2, k1)
    two = 2.0 * math.pi / inner * (np.outer(n2, n2) % inner)
    scale = 1.0 / math.sqrt(length)
    c, s, z = np.cos(two) * scale, np.sin(two) * scale, np.zeros((inner, inner))
    usual = np.block([[c, s, -s, c], [c, s, s, -c]])
    special = np.block([[c, s, z, z], [z, z, c, s]])
    return (
        first.astype(jnp.bfloat16),
        np.cos(turn).astype(np.float32),
        np.sin(turn).astype(np.float32),
        usual.astype(jnp.bfloat16),
        special.astype(jnp.bfloat16),
    )


def position_kernel(pairs, x_ref, first_ref, cos_ref, sin_ref, usual_ref, zeroth_ref, o_ref):
    outer = first_ref.shape[0]
    inner = cos_ref.shape[0]

    def turned(slot):
        a = lax.dot_general(
            x_ref[slot], first_ref[...], (((0,), (0,)), ((), ())), preferred_element_type=jnp.float32
        )
        re, im = a[:, :outer], a[:, outer:]
        c, s = cos_ref[...], sin_ref[...]
        return [(re * c + im * s).astype(jnp.bfloat16), (im * c - re * s).astype(jnp.bfloat16)]

    for pair in range(pairs):
        b = jnp.concatenate(turned(pair) + turned(pair + pairs), axis=0)
        table = zeroth_ref if pair == 0 else usual_ref
        o = jnp.dot(table[...], b, preferred_element_type=jnp.float32).astype(jnp.bfloat16)
        o_ref[pair] = o[:inner]
        o_ref[pair + pairs] = o[inner:]


def position_transform(x, zeroth_here, outer, inner):
    slots = x.shape[0]
    first, turn_cos, turn_sin, usual, special = position_tables(outer, inner)
    zeroth = jnp.where(zeroth_here, special, usual)
    return pl.pallas_call(
        functools.partial(position_kernel, slots // 2),
        out_shape=jax.ShapeDtypeStruct((slots, inner, outer), jnp.bfloat16),
        in_specs=[pl.BlockSpec(memory_space=pltpu.VMEM)] * 6,
        out_specs=pl.BlockSpec(memory_space=pltpu.VMEM),
    )(x, first, turn_cos, turn_sin, usual, zeroth)


def exchange(blocks):
    return lax.all_to_all(blocks, AXES, split_axis=0, concat_axis=0, tiled=True)


def local(tokens, norm_gain, in_weight, out_weight):
    rows_here = tokens.shape[0]
    channels = in_weight.shape[1]
    groups = channels // GROUP_WIDTH
    devices = lax.axis_size(AXES)
    me = lax.axis_index(AXES)
    slots = channels // devices
    length = rows_here * devices
    inner = 1 << ((length.bit_length()) // 2)
    outer = length // inner
    split = rows_here // inner

    forward, order = channel_tables(slots)
    floats = tokens.astype(jnp.float32)
    scaling = lax.rsqrt(jnp.mean(floats * floats, axis=-1, keepdims=True) + 1e-06)
    normed = (floats * scaling * norm_gain.astype(jnp.float32)).astype(jnp.bfloat16)
    hidden = lax.dot_general(
        in_weight, normed, (((0,), (1,)), ((), ())), preferred_element_type=jnp.float32
    ).astype(jnp.bfloat16)
    sent = jnp.einsum(
        "sc,gct->gst",
        forward,
        hidden.reshape(groups, GROUP_WIDTH, rows_here),
        preferred_element_type=jnp.float32,
    ).astype(jnp.bfloat16)
    taken = exchange(sent.reshape(devices, slots, rows_here))
    grid = taken.reshape(devices, slots, split, inner).transpose(1, 0, 2, 3)
    zeroth_here = me * (slots // 2) % (GROUP_WIDTH // 2) == 0
    done = position_transform(grid.reshape(slots, outer, inner), zeroth_here, outer, inner)
    back = done.reshape(slots, devices, rows_here // outer, outer).transpose(1, 0, 2, 3)
    returned = exchange(back.reshape(devices, slots, rows_here))
    ordered = jnp.einsum(
        "ms,gst->gmt",
        order,
        returned.reshape(groups, GROUP_WIDTH, rows_here),
        preferred_element_type=jnp.float32,
    ).astype(jnp.bfloat16)
    mixed = lax.dot_general(
        ordered.reshape(channels, rows_here),
        out_weight,
        (((0,), (0,)), ((), ())),
        preferred_element_type=jnp.float32,
    )
    return mixed.astype(jnp.bfloat16)


def solution(mesh):
    placed = (P(AXES, None), P(), P(), P())
    return jax.shard_map(
        local, mesh=mesh, in_specs=placed, out_specs=P(AXES, None), check_vma=False
    )
```

time: 137 us -> 98.7 us (0.72)
  matrix products: 40.4 us -> 20.5 us
  waiting for transfers between devices: 44 us -> 25.4 us
  Pallas kernels: 0 us -> 6.35 us
  starting transfers between devices: 11.1 us -> 7.34 us
  local copies, waits for them, and re-layouts: 7.3 us -> 4.4 us
    dot_general x9 -> x3, matrix products: 33.2 us -> 11.3 us  [the longest x1 9.51 us: local(): lax.dot_general(ordered.reshape(channels, rows_here), out_weight, (((0,),...]
    all_to_all x2 -> x1, waiting for transfers between devices: 44 us -> 25.4 us  [exchange(): return lax.all_to_all(blocks, AXES, split_axis=0, concat_axis=0, tiled=True)]
    pallas_call x0 -> x1, Pallas kernels: none -> 6.35 us  [position_transform(): pl.pallas_call(functools.partial(position_kernel, slots // 2), out_shape=...]
    all_to_all x2 -> x1, starting transfers between devices: 11.1 us -> 7.34 us  [exchange(): return lax.all_to_all(blocks, AXES, split_axis=0, concat_axis=0, tiled=True)]
    all_to_all x2 -> x0, local copies, waits for them, and re-layouts: 2.38 us -> none  [the longest x1 1.8 us: local(): lax.all_to_all(imag_chan.astype(jnp.bfloat16), ('row', 'col'), split_axis...]
    dot_general x1, matrix products: 7.19 us -> 9.23 us  [local(): lax.dot_general(in_weight, normed, (((0,), (1,)), ((), ())), preferred_el...]
    reshape x2 -> x4, local copies, waits for them, and re-layouts: 3.18 us -> 3.84 us  [the longest x2 2.05 us: local(): returned = exchange(back.reshape(devices, slots, rows_here))]
  transfers between devices with their start and end apart: 2 -> 1, of which waited for: 2 -> 1; matrix products, arithmetic and copies ran while one was open for 6% -> 1% of each run, Pallas kernels for 0% -> 0%
where the time goes in v1:
time: 98.7 us; the launch traced here: 98.3 us
  blocking collectives  29.6 us (30%)
  waiting for transfers between devices  25.4 us (26%)
  matrix products  20.5 us (21%)
  starting transfers between devices  7.34 us (7%)
  Pallas kernels  6.35 us (6%)
  other arithmetic  4.52 us (5%)
  local copies, waits for them, and re-layouts  4.4 us (4%)
    all_to_all x1, blocking collectives, exchange(): return lax.all_to_all(blocks, AXES, split_axis=0, concat_axis=0, tiled=True)  29.6 us
    all_to_all x1, waiting for transfers between devices, exchange(): return lax.all_to_all(blocks, AXES, split_axis=0, concat_axis=0, tiled=True)  25.4 us
    dot_general x1, matrix products, local(): lax.dot_general(ordered.reshape(channels, rows_here), out_weight, (((0,),...  9.51 us
    dot_general x1, matrix products, local(): lax.dot_general(in_weight, normed, (((0,), (1,)), ((), ())), preferred_el...  9.23 us
    all_to_all x1, starting transfers between devices, exchange(): return lax.all_to_all(blocks, AXES, split_axis=0, concat_axis=0, tiled=True)  7.34 us
    pallas_call x1, Pallas kernels, position_transform(): pl.pallas_call(functools.partial(position_kernel, slots // 2), out_shape=...  6.35 us
    reduce_sum x1, other arithmetic, local(): jnp.mean(floats * floats, axis=-1, keepdims=True) + 1e-06  3.08 us
    reshape x2, local copies, waits for them, and re-layouts, local(): returned = exchange(back.reshape(devices, slots, rows_here))  2.05 us
  transfers between devices with their start and end apart: 1, of which 1 were waited for; matrix products, arithmetic and copies ran while one was open for 1% of the time, Pallas kernels for 0%

profile of v1, /device:TPU:0, one launch (start us, length us, event | category | flops | bytes accessed | tf_op | source)
XLA Modules:
  0.0 98.3 jit_solution(12154562444669421842)
XLA Ops:
  0.0 3.1 %fusion = f32[512]{0:T(512)S(1)} fusion(bf16[512,4096]{1,0:T(8,128)(2,1)} %param.11), kind=kLoop, calls=%fused_computation.2 | loop fusion | flops 6290944 | bytes 4196352 | tf_op jit(solution)/shard_map/reduce_sum | solution.py:110
  3.1 0.7 convert_element_type.31
  3.8 0.0 copy-start.3
  3.8 0.0 copy-start
  3.8 0.0 copy-start.1
  3.8 9.2 %fusion.10 = bf16[1024,512]{0,1:T(8,128)(2,1)S(1)} fusion(bf16[4096,1024]{1,0:T(8,128)(2,1)} %param.13, bf16[512,4096]{1,0:T(8,128)(2,1)} %param.11, f32[4096]{0:T(1024)S(1)} %convert_element_type.31, f32[512]{0:T(512)S(1)} %add_rsqrt_fusion), kind=kOutput, calls=%fused_computation.12 | convolution fusion | flops 4303880192 | bytes 13649920 | tf_op jit(solution)/shard_map/dot_general | solution.py:112
  13.0 0.5 copy.15
  13.6 0.0 copy-done.3
  13.6 1.4 %convolution_convert_fusion.2 = bf16[16,512,64]{1,2,0:T(8,128)(2,1)} fusion(bf16[64,64,1]{1,0,2:T(8,128)(2,1)S(1)} %copy-done.3, bf16[16,64,512]{2,1,0:T(8,128)(2,1)S(1)} %bitcast.27), kind=kOutput, calls=%fused_computation.11 | convolution fusion | flops 67633152 | bytes 2105344 | tf_op jit(solution)/shard_map/sc,gct->gst/dot_general | solution.py:115
  15.0 0.0 copy-start.2
  15.0 7.3 %all-to-all-start = ((bf16[32,32,512]{2,1,0:T(8,128)(2,1)}), bf16[32,32,512]{2,1,0:T(8,128)(2,1)S(1)}, u32[]{:S(2)}, u32[]{:S(2)}) async-start(bf16[32,32,512]{2,1,0:T(8,128)(2,1)} %bitcast.4), calls=%async_computation | async-start | bytes 2097152 | tf_op jit(solution)/shard_map/all_to_all | solution.py:93
  22.3 0.0 copy-done
  22.4 0.0 copy-done.1
  22.4 0.7 broadcast_select_fusion.zeroth_ref
  23.1 25.4 %all-to-all-done = bf16[32,32,512]{2,1,0:T(8,128)(2,1)S(1)} async-done(((bf16[32,32,512]{2,1,0:T(8,128)(2,1)}), bf16[32,32,512]{2,1,0:T(8,128)(2,1)S(1)}, u32[]{:S(2)}, u32[]{:S(2)}) %all-to-all-start) | async-done | bytes 1048608 | tf_op jit(solution)/shard_map/all_to_all | solution.py:93
  48.5 0.3 reshape.43
  48.8 1.5 %copy.18 = bf16[32,32,4,128]{3,2,0,1:T(4,128)(2,1)} copy(bf16[32,32,4,128]{3,2,1,0:T(4,128)(2,1)S(1)} %reshape.43) | data formatting | bytes 2097152 | tf_op jit(solution)/shard_map/reshape | solution.py:122
  50.3 6.3 %shard_map.109 = bf16[32,128,128]{2,1,0:T(8,128)(2,1)} custom-call(bf16[32,128,128]{2,1,0:T(8,128)(2,1)} %bitcast.29, bf16[128,256]{1,0:T(8,128)(2,1)} %constant.51.clone.first_ref, f32[128,128]{1,0:T(8,128)} %constant.52.clone.cos_ref, f32[128,128]{1,0:T(8,128)} %constant.53.clone.sin_ref, bf16[256,512]{1,0:T(8,128)(2,1)} %constant.50.clone.usual_ref, ...), custom_call_target="tpu_custom_call" | custom-call | tf_op jit(solution)/shard_map/pallas_call | solution.py:84
  56.7 1.5 %reshape.38 = bf16[32,32,512]{2,0,1:T(8,128)(2,1)S(1)} reshape(bf16[32,32,4,128]{3,2,0,1:T(4,128)(2,1)} %bitcast.30) | data formatting | bytes 2097152 | tf_op jit(solution)/shard_map/reshape | solution.py:126
  58.2 0.6 copy.17
  58.7 29.6 %all_to_all.10 = bf16[32,32,512]{2,1,0:T(8,128)(2,1)S(1)} all-to-all(bf16[32,32,512]{2,1,0:T(8,128)(2,1)S(1)} %copy.17), channel_id=1, replica_groups=mesh['row'=8,'col'=4] {'row','col'}, dimensions={0} | all-to-all | bytes 2097152 | tf_op jit(solution)/shard_map/all_to_all | solution.py:93
  88.4 0.0 copy-done.2
  88.4 0.4 convolution_convert_fusion.1
  88.8 9.5 %convolution_convert_fusion = bf16[512,4096]{1,0:T(8,128)(2,1)} fusion(bf16[1024,512]{1,0:T(8,128)(2,1)S(1)} %bitcast.31, bf16[1024,4096]{1,0:T(8,128)(2,1)} %param.14), kind=kOutput, calls=%fused_computation.5 | convolution fusion | flops 4297064448 | bytes 13631488 | tf_op jit(solution)/shard_map/dot_general | solution.py:133
  (1 shorter events, 0.0 us)
Async XLA Ops:
  3.8 9.8 %copy-start.3 = (bf16[64,64,1]{1,0,2:T(8,128)(2,1)S(1)}, bf16[64,64,1]{1,0,2:T(8,128)(2,1)}, u32[]{:S(2)}) copy-start(bf16[64,64,1]{1,0,2:T(8,128)(2,1)} %constant.55) | copy-start | bytes 24580
  3.8 18.5 %copy-start = (bf16[256,512]{1,0:T(8,128)(2,1)S(1)}, bf16[256,512]{1,0:T(8,128)(2,1)}, u32[]{:S(2)}) copy-start(bf16[256,512]{1,0:T(8,128)(2,1)} %constant.50.clone.usual_ref) | copy-start | bytes 786436
  3.8 18.6 %copy-start.1 = (bf16[256,512]{1,0:T(8,128)(2,1)S(1)}, bf16[256,512]{1,0:T(8,128)(2,1)}, u32[]{:S(2)}) copy-start(bf16[256,512]{1,0:T(8,128)(2,1)} %constant.49.clone) | copy-start | bytes 786436
  15.0 73.4 %copy-start.2 = (bf16[64,64,1]{1,0,2:T(8,128)(2,1)S(1)}, bf16[64,64,1]{1,0,2:T(8,128)(2,1)}, u32[]{:S(2)}) copy-start(bf16[64,64,1]{1,0,2:T(8,128)(2,1)} %constant.56) | copy-start | bytes 24580
  15.0 33.5 %all-to-all-start = ((bf16[32,32,512]{2,1,0:T(8,128)(2,1)}), bf16[32,32,512]{2,1,0:T(8,128)(2,1)S(1)}, u32[]{:S(2)}, u32[]{:S(2)}) async-start(bf16[32,32,512]{2,1,0:T(8,128)(2,1)} %bitcast.4), calls=%async_computation | async-start | bytes 2097152 | tf_op jit(solution)/shard_map/all_to_all | solution.py:93

commit v2 on v1

--- a/solution.py
+++ b/solution.py
@@ -89,14 +89,198 @@
     )(x, first, turn_cos, turn_sin, usual, zeroth)
 
 
-def exchange(blocks):
-    return lax.all_to_all(blocks, AXES, split_axis=0, concat_axis=0, tiled=True)
+PLANES = 4
+MESH = pl.DeviceIdType.MESH
+
+
+def place_of(device, columns):
+    return (device // columns, device % columns)
+
+
+def turned_plane(plane, step):
+    high = (plane // 2 + 1 - step // 2) % 2
+    low = (plane % 2 + (step + 1) // 2) % 2
+    return 2 * high + low
+
+
+def here(devices):
+    columns = lax.axis_size("col")
+    me = lax.axis_index("row") * columns + lax.axis_index("col")
+    per = devices // PLANES
+    return me, columns, per, me // per, me % per
+
+
+def greet(devices):
+    me, columns, _, _, _ = here(devices)
+    barrier = pltpu.get_barrier_semaphore()
+
+    def signal(step, carry):
+        other = (me + step) % devices
+        pl.semaphore_signal(barrier, inc=1, device_id=place_of(other, columns), device_id_type=MESH)
+        return carry
+
+    lax.fori_loop(1, devices, signal, 0)
+    return lambda: pl.semaphore_wait(barrier, devices - 1)
+
+
+def send_plane(devices, step, from_ref, to_ref, send_sem, recv_sem, first):
+    me, columns, per, plane, lane = here(devices)
+    target_plane = turned_plane(plane, step)
+
+    def send(hop, carry):
+        target = target_plane * per + (lane + hop) % per
+        pltpu.make_async_remote_copy(
+            src_ref=from_ref.at[target],
+            dst_ref=to_ref.at[me],
+            send_sem=send_sem.at[step],
+            recv_sem=recv_sem.at[step],
+            device_id=place_of(target, columns),
+            device_id_type=MESH,
+        ).start()
+        return carry
+
+    lax.fori_loop(first, per, send, 0)
+
+
+def wait_for(ref, sem, count):
+    part = ref.at[pl.ds(0, count)]
+    pltpu.make_async_copy(part, part, sem).wait()
+
+
+def enter_kernel(
+    devices, tokens, gain, weight, forward, out, raw, normed, held, sent, token_sem, weight_sem, own_sem, send_sem, recv_sem
+):
+    me, columns, per, plane, lane = here(devices)
+    pieces = token_sem.shape[0]
+    rows = raw.shape[0]
+    piece = rows // pieces
+    width = held.shape[2]
+
+    def token_copy(index):
+        part = pl.ds(index * piece, piece)
+        return pltpu.make_async_copy(tokens.at[part], raw.at[part], token_sem.at[index])
+
+    def weight_copy(step):
+        target_plane = turned_plane(plane, step)
+        part = pl.ds(pl.multiple_of(target_plane * width, width), width)
+        return pltpu.make_async_copy(weight.at[:, part], held.at[step], weight_sem.at[step])
+
+    for index in range(pieces):
+        token_copy(index).start()
+    for step in range(PLANES):
+        weight_copy(step).start()
+    arrive = greet(devices)
+
+    block = 16
+    for index in range(pieces):
+        token_copy(index).wait()
+
+        def normalise(number, carry):
+            part = pl.ds(pl.multiple_of(index * piece + number * block, block), block)
+            floats = raw[part, :].astype(jnp.float32)
+            scaling = lax.rsqrt(jnp.mean(floats * floats, axis=-1, keepdims=True) + 1e-06)
+            normed[part, :] = (floats * scaling * gain[...].astype(jnp.float32)).astype(jnp.bfloat16)
+            return carry
+
+        lax.fori_loop(0, piece // block, normalise, 0)
+
+    arrive()
+
+    def chunk(step, carry):
+        weight_copy(step).wait()
+        target_plane = turned_plane(plane, step)
+        hidden = jnp.dot(normed[...], held[step], preferred_element_type=jnp.float32).astype(jnp.bfloat16)
+        spectrum = lax.dot_general(
+            forward[...], hidden, (((1,), (1,)), ((), ())), preferred_element_type=jnp.float32
+        )
+        sent[pl.ds(target_plane * per, per)] = spectrum.reshape(per, width // per, rows).astype(jnp.bfloat16)
+        send_plane(devices, step, sent, out, send_sem, recv_sem, step // (PLANES - 1))
+        return carry
+
+    lax.fori_loop(0, PLANES, chunk, 0)
+    own = pltpu.make_async_copy(sent.at[me], out.at[me], own_sem)
+    own.start()
+    finish(per, sent, send_sem)
+    finish(per, sent, recv_sem)
+    own.wait()
+
+
+def finish(per, ref, sem):
+    for step in range(PLANES):
+        wait_for(ref, sem.at[step], per - step // (PLANES - 1))
+
+
+def enter(tokens, gain, weight, forward, devices):
+    rows, depth = tokens.shape
+    channels = weight.shape[1]
+    slots = channels // devices
+    whole = pl.BlockSpec(memory_space=pltpu.VMEM)
+    far = pl.BlockSpec(memory_space=pl.ANY)
+    pieces = 4
+    return pl.pallas_call(
+        functools.partial(enter_kernel, devices),
+        out_shape=jax.ShapeDtypeStruct((devices, slots, rows), jnp.bfloat16),
+        in_specs=[far, whole, far, whole],
+        out_specs=far,
+        scratch_shapes=[
+            pltpu.VMEM((rows, depth), jnp.bfloat16),
+            pltpu.VMEM((rows, depth), jnp.bfloat16),
+            pltpu.VMEM((PLANES, depth, channels // PLANES), jnp.bfloat16),
+            pltpu.VMEM((devices, slots, rows), jnp.bfloat16),
+            pltpu.SemaphoreType.DMA((pieces,)),
+            pltpu.SemaphoreType.DMA((PLANES,)),
+            pltpu.SemaphoreType.DMA,
+            pltpu.SemaphoreType.DMA((PLANES,)),
+            pltpu.SemaphoreType.DMA((PLANES,)),
+        ],
+        compiler_params=pltpu.CompilerParams(collective_id=0, has_side_effects=True, vmem_limit_bytes=40 << 20),
+    )(tokens, gain.reshape(1, depth), weight, forward)
+
+
+def leave_kernel(devices, back, order, out, taken, own_sem, send_sem, recv_sem):
+    me, columns, per, plane, lane = here(devices)
+    greet(devices)()
+    for step in range(PLANES):
+        send_plane(devices, step, back, taken, send_sem, recv_sem, step // (PLANES - 1))
+    own = pltpu.make_async_copy(back.at[me], taken.at[me], own_sem)
+    own.start()
+    width = order.shape[0]
+    rows = out.shape[0]
+    own.wait()
+    for number in range(PLANES):
+        step = PLANES - 1 - number
+        wait_for(taken, recv_sem.at[step], per - step // (PLANES - 1))
+        source = turned_plane(plane, step)
+        part = taken[pl.ds(source * per, per)].astype(jnp.float32).reshape(width, rows).astype(jnp.bfloat16)
+        turned = lax.dot_general(
+            part, order[...], (((0,), (0,)), ((), ())), preferred_element_type=jnp.float32
+        ).astype(jnp.bfloat16)
+        out[:, pl.ds(pl.multiple_of(source * width, width), width)] = turned
+    finish(per, back, send_sem)
+
+
+def leave(back, order, devices):
+    _, slots, rows = back.shape
+    whole = pl.BlockSpec(memory_space=pltpu.VMEM)
+    far = pl.BlockSpec(memory_space=pl.ANY)
+    return pl.pallas_call(
+        functools.partial(leave_kernel, devices),
+        out_shape=jax.ShapeDtypeStruct((rows, devices * slots), jnp.bfloat16),
+        in_specs=[far, whole],
+        out_specs=whole,
+        scratch_shapes=[
+            pltpu.VMEM((devices, slots, rows), jnp.bfloat16),
+            pltpu.SemaphoreType.DMA,
+            pltpu.SemaphoreType.DMA((PLANES,)),
+            pltpu.SemaphoreType.DMA((PLANES,)),
+        ],
+        compiler_params=pltpu.CompilerParams(collective_id=1, has_side_effects=True, vmem_limit_bytes=16 << 20),
+    )(back, order)
 
 
 def local(tokens, norm_gain, in_weight, out_weight):
     rows_here = tokens.shape[0]
     channels = in_weight.shape[1]
-    groups = channels // GROUP_WIDTH
     devices = lax.axis_size(AXES)
     me = lax.axis_index(AXES)
     slots = channels // devices
@@ -106,37 +290,16 @@
     split = rows_here // inner
 
     forward, order = channel_tables(slots)
-    floats = tokens.astype(jnp.float32)
-    scaling = lax.rsqrt(jnp.mean(floats * floats, axis=-1, keepdims=True) + 1e-06)
-    normed = (floats * scaling * norm_gain.astype(jnp.float32)).astype(jnp.bfloat16)
-    hidden = lax.dot_general(
-        in_weight, normed, (((0,), (1,)), ((), ())), preferred_element_type=jnp.float32
-    ).astype(jnp.bfloat16)
-    sent = jnp.einsum(
-        "sc,gct->gst",
-        forward,
-        hidden.reshape(groups, GROUP_WIDTH, rows_here),
-        preferred_element_type=jnp.float32,
-    ).astype(jnp.bfloat16)
-    taken = exchange(sent.reshape(devices, slots, rows_here))
+    several = np.eye(channels // PLANES // GROUP_WIDTH)
+    forward = np.kron(several, forward.astype(np.float32)).astype(jnp.bfloat16)
+    order = np.kron(several, order.astype(np.float32)).T.astype(jnp.bfloat16)
+    taken = enter(tokens, norm_gain, in_weight, forward, devices)
     grid = taken.reshape(devices, slots, split, inner).transpose(1, 0, 2, 3)
     zeroth_here = me * (slots // 2) % (GROUP_WIDTH // 2) == 0
     done = position_transform(grid.reshape(slots, outer, inner), zeroth_here, outer, inner)
     back = done.reshape(slots, devices, rows_here // outer, outer).transpose(1, 0, 2, 3)
-    returned = exchange(back.reshape(devices, slots, rows_here))
-    ordered = jnp.einsum(
-        "ms,gst->gmt",
-        order,
-        returned.reshape(groups, GROUP_WIDTH, rows_here),
-        preferred_element_type=jnp.float32,
-    ).astype(jnp.bfloat16)
-    mixed = lax.dot_general(
-        ordered.reshape(channels, rows_here),
-        out_weight,
-        (((0,), (0,)), ((), ())),
-        preferred_element_type=jnp.float32,
-    )
-    return mixed.astype(jnp.bfloat16)
+    ordered = leave(back.reshape(devices, slots, rows_here), order, devices)
+    return jnp.dot(ordered, out_weight, preferred_element_type=jnp.float32).astype(jnp.bfloat16)
 
 
 def solution(mesh):

time: 98.7 us -> 91.2 us (0.924)
  the two profiles are of different devices: /device:TPU:0 before, /device:TPU:9 now
where the time goes in v2:
time: 91.2 us; the launch traced here: 90.8 us
  Pallas kernels  68.4 us (75%)
  local copies, waits for them, and re-layouts  11.2 us (12%)
  matrix products  9.41 us (10%)
  other arithmetic  1.69 us (2%)
    pallas_call x1, Pallas kernels, enter(): pl.pallas_call(functools.partial(enter_kernel, devices), out_shape=jax.Sh...  34.2 us
    pallas_call x1, Pallas kernels, leave(): pl.pallas_call(functools.partial(leave_kernel, devices), out_shape=jax.Sh...  27.9 us
    dot_general x1, matrix products, local(): jnp.dot(ordered, out_weight, preferred_element_type=jnp.float32)  9.41 us
    unnamed x8, local copies, waits for them, and re-layouts  6.48 us
    pallas_call x1, Pallas kernels, position_transform(): pl.pallas_call(functools.partial(position_kernel, slots // 2), out_shape=...  6.35 us

profile of v2, /device:TPU:9, one launch (start us, length us, event | category | flops | bytes accessed | tf_op | source)
XLA Modules:
  0.0 90.8 jit_solution(6727487904770912903)
XLA Ops:
  0.0 0.7 reshape.15.gain
  0.7 1.7 %broadcast_select_fusion.zeroth_ref = bf16[256,512]{1,0:T(8,128)(2,1)} fusion(bf16[256,512]{1,0:T(8,128)(2,1)} %constant.42.clone, bf16[256,512]{1,0:T(8,128)(2,1)} %constant.43.clone.usual_ref, pred[]{:T(512)S(6)} %eq.5), kind=kLoop, calls=%fused_computation.2 | loop fusion | flops 131072 | bytes 786433 | tf_op jit(solution)/shard_map/jit(_where)/select_n | solution.py:83
  2.4 0.0 copy-start
  2.4 3.4 %copy-done = bf16[4096,1024]{1,0:T(8,128)(2,1)S(1)} copy-done((bf16[4096,1024]{1,0:T(8,128)(2,1)S(1)}, bf16[4096,1024]{1,0:T(8,128)(2,1)}, u32[]{:S(2)}) %copy-start) | copy-done | bytes 8388632
  5.8 0.0 copy-start.1
  5.8 2.2 %copy-done.1 = bf16[512,4096]{1,0:T(8,128)(2,1)S(1)} copy-done((bf16[512,4096]{1,0:T(8,128)(2,1)S(1)}, bf16[512,4096]{1,0:T(8,128)(2,1)}, u32[]{:S(2)}) %copy-start.1) | copy-done | bytes 4194328
  8.0 0.0 copy-start.2
  8.0 0.9 copy-done.2
  8.9 34.2 %shard_map.109 = bf16[32,32,512]{2,1,0:T(8,128)(2,1)S(1)} custom-call(bf16[512,4096]{1,0:T(8,128)(2,1)S(1)} %copy-done.1, bf16[1,4096]{1,0:T(2,128)(2,1)S(1)} %reshape.15.gain, bf16[4096,1024]{1,0:T(8,128)(2,1)S(1)} %copy-done, bf16[256,256]{1,0:T(8,128)(2,1)S(1)} %copy-done.2), custom_call_target="tpu_custom_call" | custom-call | tf_op jit(solution)/shard_map/pallas_call | solution.py:220
  43.1 0.0 copy-start.3
  43.1 0.3 reshape.16
  43.4 1.5 %copy.12 = bf16[32,32,4,128]{3,2,0,1:T(4,128)(2,1)} copy(bf16[32,32,4,128]{3,2,1,0:T(4,128)(2,1)S(1)} %reshape.16) | data formatting | bytes 2097152 | tf_op jit(solution)/shard_map/reshape | solution.py:297
  44.9 6.4 %shard_map.110 = bf16[32,128,128]{2,1,0:T(8,128)(2,1)} custom-call(bf16[32,128,128]{2,1,0:T(8,128)(2,1)} %bitcast.10, bf16[128,256]{1,0:T(8,128)(2,1)} %constant.44.clone.first_ref, f32[128,128]{1,0:T(8,128)} %constant.45.clone.cos_ref, f32[128,128]{1,0:T(8,128)} %constant.46.clone.sin_ref, bf16[256,512]{1,0:T(8,128)(2,1)} %constant.43.clone.usual_ref, ...), custom_call_target="tpu_custom_call" | custom-call | tf_op jit(solution)/shard_map/pallas_call | solution.py:84
  51.3 1.8 %copy.15 = bf16[32,32,4,128]{3,2,0,1:T(4,128)(2,1)S(1)} copy(bf16[32,32,4,128]{3,2,1,0:T(4,128)(2,1)} %bitcast.11) | data formatting | bytes 2097152 | tf_op jit(solution)/shard_map/reshape | solution.py:300
  53.1 0.4 reshape.19.back
  53.5 0.0 copy-done.3
  53.5 27.9 %shard_map.111 = bf16[512,1024]{1,0:T(8,128)(2,1)S(1)} custom-call(bf16[32,32,512]{2,1,0:T(8,128)(2,1)S(1)} %reshape.19.back, bf16[256,256]{1,0:T(8,128)(2,1)S(1)} %copy-done.3), custom_call_target="tpu_custom_call" | custom-call | tf_op jit(solution)/shard_map/pallas_call | solution.py:266
  81.4 9.4 %convolution_convert_fusion = bf16[512,4096]{1,0:T(8,128)(2,1)} fusion(bf16[512,1024]{1,0:T(8,128)(2,1)S(1)} %shard_map.111, bf16[1024,4096]{1,0:T(8,128)(2,1)} %param.14), kind=kOutput, calls=%fused_computation | convolution fusion | flops 4297064448 | bytes 13631488 | tf_op jit(solution)/shard_map/dot_general | solution.py:302
Async XLA Ops:
  2.4 3.4 %copy-start = (bf16[4096,1024]{1,0:T(8,128)(2,1)S(1)}, bf16[4096,1024]{1,0:T(8,128)(2,1)}, u32[]{:S(2)}) copy-start(bf16[4096,1024]{1,0:T(8,128)(2,1)} %weight.1) | copy-start | bytes 25165828
  5.8 2.2 %copy-start.1 = (bf16[512,4096]{1,0:T(8,128)(2,1)S(1)}, bf16[512,4096]{1,0:T(8,128)(2,1)}, u32[]{:S(2)}) copy-start(bf16[512,4096]{1,0:T(8,128)(2,1)} %tokens.1) | copy-start | bytes 12582916
  8.0 0.9 copy-start.2
  43.1 10.4 %copy-start.3 = (bf16[256,256]{1,0:T(8,128)(2,1)S(1)}, bf16[256,256]{1,0:T(8,128)(2,1)}, u32[]{:S(2)}) copy-start(bf16[256,256]{1,0:T(8,128)(2,1)} %constant.47.clone.order) | copy-start | bytes 393220

commit v3 on v2

v3 whole, which is shorter than its diff:
```python
import functools
import math

import jax
import jax.numpy as jnp
import numpy as np
from jax import lax
from jax.experimental import pallas as pl
from jax.experimental.pallas import tpu as pltpu
from jax.sharding import PartitionSpec as P

GROUP_WIDTH = 64
AXES = ("row", "col")


def channel_tables(slots):
    pairs = slots // 2
    half = GROUP_WIDTH // 2
    index = np.arange(GROUP_WIDTH)
    forward = np.zeros((GROUP_WIDTH, GROUP_WIDTH))
    order = np.zeros((GROUP_WIDTH, GROUP_WIDTH))
    for slot in range(GROUP_WIDTH):
        place, within = divmod(slot, slots)
        pair = place * pairs + within % pairs
        angles = 2.0 * math.pi / GROUP_WIDTH * (pair * index % GROUP_WIDTH)
        if within < pairs:
            forward[slot] = np.cos(angles)
            order[pair, slot] = 1.0
        elif pair == 0:
            forward[slot] = np.cos(math.pi * index)
            order[half, slot] = 1.0
        else:
            forward[slot] = np.sin(angles)
            order[GROUP_WIDTH - pair, slot] = 1.0
    forward /= math.sqrt(GROUP_WIDTH)
    return forward.astype(jnp.bfloat16), order.astype(jnp.bfloat16)


def position_tables(outer, inner, devices):
    length = outer * inner
    k1 = np.arange(outer)
    n2 = np.arange(inner)
    n1_order = k1.reshape(devices, -1).T.reshape(-1)
    k2_order = n2.reshape(devices, -1).T.reshape(-1)
    one = 2.0 * math.pi / outer * (np.outer(n1_order, k1) % outer)
    first = np.concatenate([np.cos(one), -np.sin(one)], axis=1)
    turn = 2.0 * math.pi / length * np.outer(n2, k1)
    two = 2.0 * math.pi / inner * (np.outer(k2_order, n2) % inner)
    scale = 1.0 / math.sqrt(length)
    c, s, z = np.cos(two) * scale, np.sin(two) * scale, np.zeros((inner, inner))
    usual = np.block([[c, s, -s, c], [c, s, s, -c]])
    zeroth = np.block([[c, s, z, z], [z, z, c, s]])
    return (
        first.astype(jnp.bfloat16),
        np.cos(turn).astype(np.float32),
        np.sin(turn).astype(np.float32),
        usual.astype(jnp.bfloat16),
        zeroth.astype(jnp.bfloat16),
    )


PLANES = 4
MESH = pl.DeviceIdType.MESH


def place_of(device, columns):
    return (device // columns, device % columns)


def turned_plane(plane, step):
    high = (plane // 2 + 1 - step // 2) % 2
    low = (plane % 2 + (step + 1) // 2) % 2
    return 2 * high + low


def here(devices):
    columns = lax.axis_size("col")
    me = lax.axis_index("row") * columns + lax.axis_index("col")
    per = devices // PLANES
    return me, columns, per, me // per, me % per


def greet(devices):
    me, columns, _, _, _ = here(devices)
    barrier = pltpu.get_barrier_semaphore()

    def signal(step, carry):
        other = (me + step) % devices
        pl.semaphore_signal(barrier, inc=1, device_id=place_of(other, columns), device_id_type=MESH)
        return carry

    lax.fori_loop(1, devices, signal, 0)
    return lambda: pl.semaphore_wait(barrier, devices - 1)


def send_plane(devices, step, from_ref, to_ref, send_sem, recv_sem, first):
    me, columns, per, plane, lane = here(devices)
    target_plane = turned_plane(plane, step)

    def send(hop, carry):
        target = target_plane * per + (lane + hop) % per
        pltpu.make_async_remote_copy(
            src_ref=from_ref.at[target],
            dst_ref=to_ref.at[me],
            send_sem=send_sem,
            recv_sem=recv_sem,
            device_id=place_of(target, columns),
            device_id_type=MESH,
        ).start()
        return carry

    lax.fori_loop(first, per, send, 0)


def wait_for(ref, sem, count):
    part = ref.at[pl.ds(0, count)]
    pltpu.make_async_copy(part, part, sem).wait()


def enter_kernel(
    devices, tokens, gain, weight, forward, out, raw, normed, held, sent, wide, token_sem, weight_sem, own_sem, send_sem, recv_sem
):
    me, columns, per, plane, lane = here(devices)
    pieces = token_sem.shape[0]
    rows = raw.shape[0]
    piece = rows // pieces
    width = held.shape[2]

    def token_copy(index):
        part = pl.ds(index * piece, piece)
        return pltpu.make_async_copy(tokens.at[part], raw.at[part], token_sem.at[index])

    def weight_copy(step):
        target_plane = turned_plane(plane, step)
        part = pl.ds(pl.multiple_of(target_plane * width, width), width)
        return pltpu.make_async_copy(weight.at[:, part], held.at[step], weight_sem.at[step])

    for index in range(pieces):
        token_copy(index).start()
    for step in range(PLANES):
        weight_copy(step).start()
    arrive = greet(devices)

    wide[...] = gain[...].astype(jnp.float32).reshape(wide.shape)
    block = 16
    for index in range(pieces):
        token_copy(index).wait()

        def normalise(number, carry):
            part = pl.ds(pl.multiple_of(index * piece + number * block, block), block)
            floats = raw[part, :].astype(jnp.float32)
            scaling = lax.rsqrt(jnp.mean(floats * floats, axis=-1, keepdims=True) + 1e-06)
            normed[part, :] = (floats * scaling * wide[...]).astype(jnp.bfloat16)
            return carry

        lax.fori_loop(0, piece // block, normalise, 0)

    arrive()

    def chunk(step, carry):
        weight_copy(step).wait()
        target_plane = turned_plane(plane, step)
        hidden = jnp.dot(normed[...], held[step], preferred_element_type=jnp.float32).astype(jnp.bfloat16)
        spectrum = lax.dot_general(
            forward[...], hidden, (((1,), (1,)), ((), ())), preferred_element_type=jnp.float32
        )
        sent[pl.ds(target_plane * per, per)] = spectrum.reshape(per, width // per, rows).astype(jnp.bfloat16)
        send_plane(devices, step, sent, out, send_sem.at[step], recv_sem.at[step], step // (PLANES - 1))
        return carry

    lax.fori_loop(0, PLANES, chunk, 0)
    own = pltpu.make_async_copy(sent.at[me], out.at[me], own_sem)
    own.start()
    finish(per, sent, send_sem)
    finish(per, sent, recv_sem)
    own.wait()


def finish(per, ref, sem):
    for step in range(PLANES):
        wait_for(ref, sem.at[step], per - step // (PLANES - 1))


def enter(tokens, gain, weight, forward, devices):
    rows, depth = tokens.shape
    channels = weight.shape[1]
    slots = channels // devices
    whole = pl.BlockSpec(memory_space=pltpu.VMEM)
    hbm = pl.BlockSpec(memory_space=pltpu.HBM)
    pieces = 4
    return pl.pallas_call(
        functools.partial(enter_kernel, devices),
        out_shape=jax.ShapeDtypeStruct((devices, slots, rows), jnp.bfloat16),
        in_specs=[hbm, whole, hbm, whole],
        out_specs=pl.BlockSpec(memory_space=pl.ANY),
        scratch_shapes=[
            pltpu.VMEM((rows, depth), jnp.bfloat16),
            pltpu.VMEM((rows, depth), jnp.bfloat16),
            pltpu.VMEM((PLANES, depth, channels // PLANES), jnp.bfloat16),
            pltpu.VMEM((devices, slots, rows), jnp.bfloat16),
            pltpu.VMEM((1, depth), jnp.float32),
            pltpu.SemaphoreType.DMA((pieces,)),
            pltpu.SemaphoreType.DMA((PLANES,)),
            pltpu.SemaphoreType.DMA,
            pltpu.SemaphoreType.DMA((PLANES,)),
            pltpu.SemaphoreType.DMA((PLANES,)),
        ],
        compiler_params=pltpu.CompilerParams(collective_id=0, has_side_effects=True, vmem_limit_bytes=61 << 20),
    )(tokens, gain, weight, forward)


def leave_kernel(
    devices,
    taken,
    first,
    turn_cos,
    turn_sin,
    usual,
    special,
    order,
    out,
    table,
    grid,
    done,
    back,
    landed,
    own_sem,
    send_sem,
    recv_sem,
):
    me, columns, per, plane, lane = here(devices)
    arrive = greet(devices)
    units, _, slots, rows = back.shape
    pairs = slots // 2
    outer = first.shape[0]
    inner = turn_cos.shape[0]

    def turned(slot):
        a = lax.dot_general(
            grid[slot], first[...], (((0,), (0,)), ((), ())), preferred_element_type=jnp.float32
        )
        re, im = a[:, :outer], a[:, outer:]
        c, s = turn_cos[...], turn_sin[...]
        return [(re * c + im * s).astype(jnp.bfloat16), (im * c - re * s).astype(jnp.bfloat16)]

    for unit in range(units):
        zeroth_here = ((me * units + unit) * pairs) % (GROUP_WIDTH // 2) == 0

        @pl.when(zeroth_here)
        def _():
            table[...] = special[...]

        @pl.when(jnp.logical_not(zeroth_here))
        def _():
            table[...] = usual[...]

        for part in range(outer // devices):
            block = taken[:, unit * slots : (unit + 1) * slots, part * inner : (part + 1) * inner]
            grid[:, part * devices : (part + 1) * devices, :] = jnp.swapaxes(
                block.astype(jnp.float32), 0, 1
            ).astype(jnp.bfloat16)
        for pair in range(pairs):
            b = jnp.concatenate(turned(pair) + turned(pair + pairs), axis=0)
            here_table = table if pair == 0 else usual
            o = jnp.dot(here_table[...], b, preferred_element_type=jnp.float32)
            done[pair] = o[:inner]
            done[pair + pairs] = o[inner:]
        for part in range(inner // devices):
            block = done[:, part * devices : (part + 1) * devices, :]
            back[unit, :, :, part * outer : (part + 1) * outer] = jnp.swapaxes(block, 0, 1).astype(jnp.bfloat16)
        if unit == 0:
            arrive()
        for step in range(PLANES):
            send_plane(
                devices,
                step,
                back.at[unit],
                landed.at[unit],
                send_sem.at[unit, step],
                recv_sem.at[unit, step],
                step // (PLANES - 1),
            )
        pltpu.make_async_copy(back.at[unit, me], landed.at[unit, me], own_sem.at[unit]).start()

    width = order.shape[0]
    for unit in range(units):
        pltpu.make_async_copy(back.at[unit, me], landed.at[unit, me], own_sem.at[unit]).wait()
    for number in range(PLANES):
        step = PLANES - 1 - number
        source = turned_plane(plane, step)
        parts = []
        for unit in range(units):
            wait_for(landed.at[unit], recv_sem.at[unit, step], per - step // (PLANES - 1))
        for unit in range(units):
            parts.append(landed[unit, pl.ds(source * per, per)].astype(jnp.float32))
        joined = jnp.concatenate(parts, axis=1).reshape(width, rows).astype(jnp.bfloat16)
        turned_back = lax.dot_general(
            joined, order[...], (((0,), (0,)), ((), ())), preferred_element_type=jnp.float32
        ).astype(jnp.bfloat16)
        out[:, pl.ds(pl.multiple_of(source * width, width), width)] = turned_back
    for unit in range(units):
        for step in range(PLANES):
            wait_for(back.at[unit], send_sem.at[unit, step], per - step // (PLANES - 1))


def leave(taken, tables, order, units, devices):
    _, all_slots, rows = taken.shape
    slots = all_slots // units
    outer = tables[0].shape[0]
    inner = tables[1].shape[0]
    whole = pl.BlockSpec(memory_space=pltpu.VMEM)
    return pl.pallas_call(
        functools.partial(leave_kernel, devices),
        out_shape=jax.ShapeDtypeStruct((rows, devices * all_slots), jnp.bfloat16),
        in_specs=[whole] * 7,
        out_specs=whole,
        scratch_shapes=[
            pltpu.VMEM(tables[3].shape, jnp.bfloat16),
            pltpu.VMEM((slots, outer, inner), jnp.bfloat16),
            pltpu.VMEM((slots, inner, outer), jnp.float32),
            pltpu.VMEM((units, devices, slots, rows), jnp.bfloat16),
            pltpu.VMEM((units, devices, slots, rows), jnp.bfloat16),
            pltpu.SemaphoreType.DMA((units,)),
            pltpu.SemaphoreType.DMA((units, PLANES)),
            pltpu.SemaphoreType.DMA((units, PLANES)),
        ],
        compiler_params=pltpu.CompilerParams(collective_id=1, has_side_effects=True, vmem_limit_bytes=20 << 20),
        cost_estimate=pl.CostEstimate(flops=20 * 10**9, bytes_accessed=50 * 2**20, transcendentals=0),
    )(taken, *tables, order)


def local(tokens, norm_gain, in_weight, out_weight):
    rows_here = tokens.shape[0]
    channels = in_weight.shape[1]
    devices = lax.axis_size(AXES)
    slots = channels // devices
    units = max(1, slots // 16)
    length = rows_here * devices
    inner = 1 << ((length.bit_length()) // 2)
    outer = length // inner

    forward, order = channel_tables(slots // units)
    several = np.eye(channels // PLANES // GROUP_WIDTH)
    forward = np.kron(several, forward.astype(np.float32)).astype(jnp.bfloat16)
    order = np.kron(several, order.astype(np.float32)).T.astype(jnp.bfloat16)
    taken = enter(tokens, norm_gain, in_weight, forward, devices)
    ordered = leave(taken, position_tables(outer, inner, devices), order, units, devices)
    return jnp.dot(ordered, out_weight, preferred_element_type=jnp.float32).astype(jnp.bfloat16)


def solution(mesh):
    placed = (P(AXES, None), P(), P(), P())
    return jax.shard_map(
        local, mesh=mesh, in_specs=placed, out_specs=P(AXES, None), check_vma=False
    )
```

time: 91.2 us -> 70.3 us (0.77)
  the two profiles are of different devices: /device:TPU:9 before, /device:TPU:0 now
where the time goes in v3:
time: 70.3 us; the launch traced here: 69.3 us
  Pallas kernels  61.9 us (88%)
  matrix products  6.08 us (9%)
  local copies, waits for them, and re-layouts  1.25 us (2%)
    pallas_call x1, Pallas kernels, enter(): pl.pallas_call(functools.partial(enter_kernel, devices), out_shape=jax.Sh...  32.2 us
    pallas_call x1, Pallas kernels, leave(): pl.pallas_call(functools.partial(leave_kernel, devices), out_shape=jax.Sh...  29.7 us
    dot_general x1, matrix products, local(): jnp.dot(ordered, out_weight, preferred_element_type=jnp.float32)  6.08 us

profile of v3, /device:TPU:0, one launch (start us, length us, event | category | flops | bytes accessed | tf_op | source)
XLA Modules:
  0.0 69.3 jit_solution(12022248669264555876)
XLA Ops:
  0.0 0.0 copy-start.3
  0.0 0.0 copy-start.1
  0.0 0.0 copy-start.2
  0.0 0.0 copy-start.4
  0.0 0.0 copy-start.5
  0.0 0.0 copy-start.6
  0.0 32.2 %shard_map.109.taken = bf16[32,32,512]{2,1,0:T(8,128)(2,1)} custom-call(bf16[512,4096]{1,0:T(8,128)(2,1)} %tokens.1, bf16[4096]{0:T(1024)(128)(2,1)} %gain.1, bf16[4096,1024]{1,0:T(8,128)(2,1)} %weight.1, bf16[256,256]{1,0:T(8,128)(2,1)} %constant.14.clone.forward), custom_call_target="tpu_custom_call" | custom-call | tf_op jit(solution)/shard_map/pallas_call | solution.py:191
  32.3 0.0 copy-done.3
  32.3 0.0 copy-done.1
  32.3 0.0 copy-done.2
  32.3 0.0 copy-done.4
  32.3 0.0 copy-done.5
  32.3 0.0 copy-done.6
  32.3 0.0 copy-start
  32.4 1.2 %copy-done = bf16[32,32,512]{2,1,0:T(8,128)(2,1)S(1)} copy-done((bf16[32,32,512]{2,1,0:T(8,128)(2,1)S(1)}, bf16[32,32,512]{2,1,0:T(8,128)(2,1)}, u32[]{:S(2)}) %copy-start) | copy-done | bytes 1048600
  33.6 0.0 copy-start.7
  33.6 29.7 %shard_map.110 = bf16[512,1024]{1,0:T(8,128)(2,1)S(1)} custom-call(bf16[32,32,512]{2,1,0:T(8,128)(2,1)S(1)} %copy-done, bf16[128,256]{1,0:T(8,128)(2,1)S(1)} %copy-done.6, f32[128,128]{1,0:T(8,128)S(1)} %copy-done.5, f32[128,128]{1,0:T(8,128)S(1)} %copy-done.4, bf16[256,512]{1,0:T(8,128)(2,1)S(1)} %copy-done.2, bf16[256,512]{1,0:T(8,128)(2,1)S(1)} %copy-done.1, ...), custom_call_target="tpu_custom_call" | custom-call | flops 20000000000 | bytes 52428800 | tf_op jit(solution)/shard_map/pallas_call | solution.py:312
  63.2 0.0 copy-done.7
  63.2 6.1 %convolution_convert_fusion = bf16[512,4096]{1,0:T(8,128)(2,1)} fusion(bf16[512,1024]{1,0:T(8,128)(2,1)S(1)} %shard_map.110, bf16[1024,4096]{1,0:T(8,128)(2,1)S(1)} %copy-done.7), kind=kOutput, calls=%fused_computation | convolution fusion | flops 4297064448 | bytes 13631488 | tf_op jit(solution)/shard_map/dot_general | solution.py:348
Async XLA Ops:
  0.0 32.3 %copy-start.3 = (bf16[256,256]{1,0:T(8,128)(2,1)S(1)}, bf16[256,256]{1,0:T(8,128)(2,1)}, u32[]{:S(2)}) copy-start(bf16[256,256]{1,0:T(8,128)(2,1)} %constant.20.clone.order) | copy-start | bytes 393220
  0.0 32.3 %copy-start.1 = (bf16[256,512]{1,0:T(8,128)(2,1)S(1)}, bf16[256,512]{1,0:T(8,128)(2,1)}, u32[]{:S(2)}) copy-start(bf16[256,512]{1,0:T(8,128)(2,1)} %constant.19.clone.special) | copy-start | bytes 786436
  0.0 32.3 %copy-start.2 = (bf16[256,512]{1,0:T(8,128)(2,1)S(1)}, bf16[256,512]{1,0:T(8,128)(2,1)}, u32[]{:S(2)}) copy-start(bf16[256,512]{1,0:T(8,128)(2,1)} %constant.18.clone.usual) | copy-start | bytes 786436
  0.0 32.3 %copy-start.4 = (f32[128,128]{1,0:T(8,128)S(1)}, f32[128,128]{1,0:T(8,128)}, u32[]{:S(2)}) copy-start(f32[128,128]{1,0:T(8,128)} %constant.17.clone.turn_sin) | copy-start | bytes 196612
  0.0 32.3 %copy-start.5 = (f32[128,128]{1,0:T(8,128)S(1)}, f32[128,128]{1,0:T(8,128)}, u32[]{:S(2)}) copy-start(f32[128,128]{1,0:T(8,128)} %constant.16.clone.turn_cos) | copy-start | bytes 196612
  0.0 32.3 %copy-start.6 = (bf16[128,256]{1,0:T(8,128)(2,1)S(1)}, bf16[128,256]{1,0:T(8,128)(2,1)}, u32[]{:S(2)}) copy-start(bf16[128,256]{1,0:T(8,128)(2,1)} %constant.15.clone.first) | copy-start | bytes 196612
  32.3 1.2 %copy-start = (bf16[32,32,512]{2,1,0:T(8,128)(2,1)S(1)}, bf16[32,32,512]{2,1,0:T(8,128)(2,1)}, u32[]{:S(2)}) copy-start(bf16[32,32,512]{2,1,0:T(8,128)(2,1)} %shard_map.109.taken) | copy-start | bytes 3145732
  33.6 29.7 %copy-start.7 = (bf16[1024,4096]{1,0:T(8,128)(2,1)S(1)}, bf16[1024,4096]{1,0:T(8,128)(2,1)}, u32[]{:S(2)}) copy-start(bf16[1024,4096]{1,0:T(8,128)(2,1)} %param.14) | copy-start | bytes 25165828

commit v4 on v3

--- a/solution.py
+++ b/solution.py
@@ -137,14 +137,13 @@
 
     for index in range(pieces):
         token_copy(index).start()
-    for step in range(PLANES):
-        weight_copy(step).start()
     arrive = greet(devices)
 
     wide[...] = gain[...].astype(jnp.float32).reshape(wide.shape)
     block = 16
     for index in range(pieces):
         token_copy(index).wait()
+        weight_copy(index).start()
 
         def normalise(number, carry):
             part = pl.ds(pl.multiple_of(index * piece + number * block, block), block)
@@ -187,7 +186,7 @@
     slots = channels // devices
     whole = pl.BlockSpec(memory_space=pltpu.VMEM)
     hbm = pl.BlockSpec(memory_space=pltpu.HBM)
-    pieces = 4
+    pieces = PLANES
     return pl.pallas_call(
         functools.partial(enter_kernel, devices),
         out_shape=jax.ShapeDtypeStruct((devices, slots, rows), jnp.bfloat16),
@@ -205,7 +204,7 @@
             pltpu.SemaphoreType.DMA((PLANES,)),
             pltpu.SemaphoreType.DMA((PLANES,)),
         ],
-        compiler_params=pltpu.CompilerParams(collective_id=0, has_side_effects=True, vmem_limit_bytes=61 << 20),
+        compiler_params=pltpu.CompilerParams(collective_id=0, has_side_effects=True, vmem_limit_bytes=60 << 20),
     )(tokens, gain, weight, forward)
 
 

time: 70.3 us -> 70.3 us (level)
  no operation moved by 1% of the time
where the time goes in v4:
time: 70.3 us; the launch traced here: 69.3 us
  Pallas kernels  61.9 us (88%)
  matrix products  6.08 us (9%)
  local copies, waits for them, and re-layouts  1.25 us (2%)
    pallas_call x1, Pallas kernels, enter(): pl.pallas_call(functools.partial(enter_kernel, devices), out_shape=jax.Sh...  32.3 us
    pallas_call x1, Pallas kernels, leave(): pl.pallas_call(functools.partial(leave_kernel, devices), out_shape=jax.Sh...  29.7 us
    dot_general x1, matrix products, local(): jnp.dot(ordered, out_weight, preferred_element_type=jnp.float32)  6.08 us

profile of v4, /device:TPU:0, one launch (start us, length us, event | category | flops | bytes accessed | tf_op | source)
XLA Modules:
  0.0 69.3 jit_solution(4799695746161705945)
XLA Ops:
  0.0 0.0 copy-start.3
  0.0 0.0 copy-start.1
  0.0 0.0 copy-start.2
  0.0 0.0 copy-start.4
  0.0 0.0 copy-start.5
  0.0 0.0 copy-start.6
  0.0 32.3 %shard_map.109.taken = bf16[32,32,512]{2,1,0:T(8,128)(2,1)} custom-call(bf16[512,4096]{1,0:T(8,128)(2,1)} %tokens.1, bf16[4096]{0:T(1024)(128)(2,1)} %gain.1, bf16[4096,1024]{1,0:T(8,128)(2,1)} %weight.1, bf16[256,256]{1,0:T(8,128)(2,1)} %constant.14.clone.forward), custom_call_target="tpu_custom_call" | custom-call | tf_op jit(solution)/shard_map/pallas_call | solution.py:190
  32.3 0.0 copy-done.3
  32.3 0.0 copy-done.1
  32.3 0.0 copy-done.2
  32.3 0.0 copy-done.4
  32.3 0.0 copy-done.5
  32.3 0.0 copy-done.6
  32.4 0.0 copy-start
  32.4 1.2 %copy-done = bf16[32,32,512]{2,1,0:T(8,128)(2,1)S(1)} copy-done((bf16[32,32,512]{2,1,0:T(8,128)(2,1)S(1)}, bf16[32,32,512]{2,1,0:T(8,128)(2,1)}, u32[]{:S(2)}) %copy-start) | copy-done | bytes 1048600
  33.6 0.0 copy-start.7
  33.6 29.7 %shard_map.110 = bf16[512,1024]{1,0:T(8,128)(2,1)S(1)} custom-call(bf16[32,32,512]{2,1,0:T(8,128)(2,1)S(1)} %copy-done, bf16[128,256]{1,0:T(8,128)(2,1)S(1)} %copy-done.6, f32[128,128]{1,0:T(8,128)S(1)} %copy-done.5, f32[128,128]{1,0:T(8,128)S(1)} %copy-done.4, bf16[256,512]{1,0:T(8,128)(2,1)S(1)} %copy-done.2, bf16[256,512]{1,0:T(8,128)(2,1)S(1)} %copy-done.1, ...), custom_call_target="tpu_custom_call" | custom-call | flops 20000000000 | bytes 52428800 | tf_op jit(solution)/shard_map/pallas_call | solution.py:311
  63.2 0.0 copy-done.7
  63.3 6.1 %convolution_convert_fusion = bf16[512,4096]{1,0:T(8,128)(2,1)} fusion(bf16[512,1024]{1,0:T(8,128)(2,1)S(1)} %shard_map.110, bf16[1024,4096]{1,0:T(8,128)(2,1)S(1)} %copy-done.7), kind=kOutput, calls=%fused_computation | convolution fusion | flops 4297064448 | bytes 13631488 | tf_op jit(solution)/shard_map/dot_general | solution.py:347
Async XLA Ops:
  0.0 32.3 %copy-start.3 = (bf16[256,256]{1,0:T(8,128)(2,1)S(1)}, bf16[256,256]{1,0:T(8,128)(2,1)}, u32[]{:S(2)}) copy-start(bf16[256,256]{1,0:T(8,128)(2,1)} %constant.20.clone.order) | copy-start | bytes 393220
  0.0 32.3 %copy-start.1 = (bf16[256,512]{1,0:T(8,128)(2,1)S(1)}, bf16[256,512]{1,0:T(8,128)(2,1)}, u32[]{:S(2)}) copy-start(bf16[256,512]{1,0:T(8,128)(2,1)} %constant.19.clone.special) | copy-start | bytes 786436
  0.0 32.3 %copy-start.2 = (bf16[256,512]{1,0:T(8,128)(2,1)S(1)}, bf16[256,512]{1,0:T(8,128)(2,1)}, u32[]{:S(2)}) copy-start(bf16[256,512]{1,0:T(8,128)(2,1)} %constant.18.clone.usual) | copy-start | bytes 786436
  0.0 32.3 %copy-start.4 = (f32[128,128]{1,0:T(8,128)S(1)}, f32[128,128]{1,0:T(8,128)}, u32[]{:S(2)}) copy-start(f32[128,128]{1,0:T(8,128)} %constant.17.clone.turn_sin) | copy-start | bytes 196612
  0.0 32.3 %copy-start.5 = (f32[128,128]{1,0:T(8,128)S(1)}, f32[128,128]{1,0:T(8,128)}, u32[]{:S(2)}) copy-start(f32[128,128]{1,0:T(8,128)} %constant.16.clone.turn_cos) | copy-start | bytes 196612
  0.0 32.3 %copy-start.6 = (bf16[128,256]{1,0:T(8,128)(2,1)S(1)}, bf16[128,256]{1,0:T(8,128)(2,1)}, u32[]{:S(2)}) copy-start(bf16[128,256]{1,0:T(8,128)(2,1)} %constant.15.clone.first) | copy-start | bytes 196612
  32.4 1.2 %copy-start = (bf16[32,32,512]{2,1,0:T(8,128)(2,1)S(1)}, bf16[32,32,512]{2,1,0:T(8,128)(2,1)}, u32[]{:S(2)}) copy-start(bf16[32,32,512]{2,1,0:T(8,128)(2,1)} %shard_map.109.taken) | copy-start | bytes 3145732
  33.6 29.7 %copy-start.7 = (bf16[1024,4096]{1,0:T(8,128)(2,1)S(1)}, bf16[1024,4096]{1,0:T(8,128)(2,1)}, u32[]{:S(2)}) copy-start(bf16[1024,4096]{1,0:T(8,128)(2,1)} %param.14) | copy-start | bytes 25165828
